TPU v7x, 32 devices: a whole 2x2x4 slice. The times are simulated.
32 devices in a mesh: rep: 2 (over x), fs: 8 (over z, y), tp: 2 (over core).
Axes of the slice: x: 2, y: 2, z: 4, core: 2. Of those that a mesh axis runs over, the one named last changes fastest.
Arguments:
- tokens: bfloat16 [4096, 1024], P(('rep', 'fs', 'tp')), may hold values from -4 to 4
- mixer_out: bfloat16 [4096, 1024], P(('rep', 'fs')), may hold values from -4 to 4
- gain_first: float32 [1024], replicated, may hold values from 0.1 to 1.9
- gate_first: bfloat16 [1024, 2816], P('fs', 'tp'), may hold values from -0.1875 to 0.1875
- up_first: bfloat16 [1024, 2816], P('fs', 'tp'), may hold values from -0.1875 to 0.1875
- down_first: bfloat16 [2816, 1024], P('tp', 'fs'), may hold values from -0.109375 to 0.109375
- gain_second: float32 [1024], replicated, may hold values from 0.1 to 1.9
- gate_second: bfloat16 [1024, 2816], P('fs', 'tp'), may hold values from -0.1875 to 0.1875
- up_second: bfloat16 [1024, 2816], P('fs', 'tp'), may hold values from -0.1875 to 0.1875
- down_second: bfloat16 [2816, 1024], P('tp', 'fs'), may hold values from -0.109375 to 0.109375
- gain_last: float32 [1024], P('tp'), may hold values from 0.1 to 1.9
Outputs:
- result: bfloat16 [4096, 1024], P(('rep', 'fs'), 'tp')
All inputs are finite; a program needn't handle non-finite values.
Results may differ from a plain program's by a relative error of at most 0.02.
Values may be sent and summed in bfloat16 or wider, within the bound.
A program may use at most 64 MiB of HBM per device.

v0:
```python
import jax
import jax.numpy as jnp
from jax import lax
from jax.sharding import PartitionSpec as P

EPS = 1e-06


def over_all(slab, axis, dim):

    def gathered(part):
        return lax.all_gather(part, axis, axis=dim, tiled=True)

    return jax.tree.map(gathered, slab)


def normalize(floats_in, gain_vec):
    floats = floats_in.astype(jnp.float32)
    factor = lax.rsqrt(jnp.mean(floats * floats, axis=-1, keepdims=True) + EPS)
    return (floats * factor * gain_vec.astype(jnp.float32)).astype(jnp.bfloat16)


def gather_group(row_block):
    return lax.all_gather(row_block, "tp", axis=0, tiled=True)


def inner_hidden(normed, w_gate, w_up):

    def add_both(totals, pieces):
        columns = lax.slice_in_dim(normed, 0, pieces[0].shape[0], axis=1)
        return (
            totals[0] + jnp.dot(columns, pieces[0], preferred_element_type=jnp.float32),
            totals[1] + jnp.dot(columns, pieces[1], preferred_element_type=jnp.float32),
        )

    empty = jnp.zeros((normed.shape[0], w_gate.shape[1]), jnp.float32)
    gate_acc, up_acc = add_both((empty, empty), over_all((w_gate, w_up), "fs", 0))
    return (jax.nn.silu(gate_acc) * up_acc).astype(jnp.bfloat16)


def outer_weight(w_down):
    return lax.all_gather(w_down, "fs", axis=1, tiled=True)


def local(
    tokens,
    mixer_out,
    gain_first,
    gate_first,
    up_first,
    down_first,
    gain_second,
    gate_second,
    up_second,
    down_second,
    gain_last,
):
    rows_dev = tokens.shape[0]
    tp_count = lax.axis_size("tp")
    tp_index = lax.axis_index("tp")
    normed_own = normalize(tokens, gain_first)
    normed_one = gather_group(normed_own)
    hidden_one = inner_hidden(normed_one, gate_first, up_first)
    down_full = outer_weight(down_first)

    def row_terms():
        picked = lax.slice_in_dim(hidden_one, 0, rows_dev * lax.axis_size("tp"), axis=0)
        return jnp.dot(picked, down_full, preferred_element_type=jnp.float32)

    ffn_one = lax.psum_scatter(
        row_terms().astype(jnp.bfloat16), "tp", scatter_dimension=0, tiled=True
    ).astype(jnp.float32)
    after_one = (tokens.astype(jnp.float32) + 0.5 * ffn_one).astype(jnp.bfloat16)
    own_mixer = lax.dynamic_slice_in_dim(mixer_out, tp_index * rows_dev, rows_dev, 0)
    mixed_in = (after_one.astype(jnp.float32) + own_mixer.astype(jnp.float32)).astype(jnp.bfloat16)
    gathered = gather_group(mixed_in)
    normed_two = normalize(gathered, gain_second)
    hidden_two = inner_hidden(normed_two, gate_second, up_second)
    down_two_full = outer_weight(down_second)
    terms_two = jnp.dot(hidden_two, down_two_full, preferred_element_type=jnp.float32)
    ffn_two = lax.psum_scatter(
        terms_two.astype(jnp.bfloat16), "tp", scatter_dimension=1, tiled=True
    ).astype(jnp.float32)
    col_width = ffn_two.shape[1]
    my_cols = lax.dynamic_slice_in_dim(gathered, tp_index * col_width, col_width, 1)
    after_two = (my_cols.astype(jnp.float32) + 0.5 * ffn_two).astype(jnp.bfloat16)
    floats = after_two.astype(jnp.float32)
    sum_sq = lax.psum(jnp.sum(floats * floats, axis=1), "tp")
    factor = lax.rsqrt(sum_sq / (col_width * tp_count) + EPS)
    return (floats * factor[:, None] * gain_last.astype(jnp.float32)[None, :]).astype(jnp.bfloat16)


def solution(mesh):
    in_specs = (
        P(("rep", "fs", "tp"), None),
        P(("rep", "fs"), None),
        P(),
        P("fs", "tp"),
        P("fs", "tp"),
        P("tp", "fs"),
        P(),
        P("fs", "tp"),
        P("fs", "tp"),
        P("tp", "fs"),
        P("tp"),
    )
    out_specs = P(("rep", "fs"), "tp")
    return jax.shard_map(local, mesh=mesh, in_specs=in_specs, out_specs=out_specs, check_vma=False)
```

profile of v0, /device:TPU:0, one launch (start us, length us, event | category | flops | bytes accessed | tf_op | source)
XLA Modules:
  0.0 402.3 jit_solution(16282262251810732455)
XLA Ops:
  6.5 0.7 all-gather.7.cloned.1.call-update
  7.3 0.7 all-gather.11.cloned.1.call-update
  8.0 0.0 all-gather.9.cloned.1.call-start
  8.1 0.7 all-gather.9.cloned.1.call-update
  8.7 0.0 reduce-scatter.3.cloned.1.call-start
  8.8 1.1 fusion.10
  9.9 1.1 fusion.12
  11.0 2.3 all_gather.24
  13.3 56.3 %all-gather.7.cloned.1.call-done = bf16[1024,1408]{1,0:T(8,128)(2,1)} async-done(((bf16[128,1408]{1,0:T(8,128)(2,1)}), bf16[1024,1408]{1,0:T(8,128)(2,1)}) %all-gather.7.cloned.1.call-update) | async-done | bytes 2883600 | tf_op jit(solution)/shard_map/all_gather | solution.py:12
  69.6 2.8 fusion.20
  72.4 57.4 %all-gather.11.cloned.1.call-done = bf16[1408,1024]{1,0:T(8,128)(2,1)} async-done(((bf16[1408,128]{1,0:T(8,128)(2,1)}), bf16[1408,1024]{1,0:T(8,128)(2,1)}) %all-gather.11.cloned.1.call-update) | async-done | bytes 2883600 | tf_op jit(solution)/shard_map/all_gather | solution.py:42
  129.8 57.7 %all-gather.9.cloned.1.call-done = bf16[1024,1408]{1,0:T(8,128)(2,1)} async-done(((bf16[128,1408]{1,0:T(8,128)(2,1)}), bf16[1024,1408]{1,0:T(8,128)(2,1)}) %all-gather.9.cloned.1.call-update) | async-done | bytes 2883600 | tf_op jit(solution)/shard_map/all_gather | solution.py:12
  187.5 5.4 %convolution_convert_fusion.1 = bf16[256,1024]{1,0:T(8,128)(2,1)} fusion(bf16[1408,1024]{1,0:T(8,128)(2,1)} %all-gather.11.cloned.1.call-done, bf16[256,1024]{1,0:T(8,128)(2,1)S(1)} %all_gather.24, bf16[1024,1408]{1,0:T(8,128)(2,1)} %all-gather.9.cloned.1.call-done, f32[256,1408]{1,0:T(8,128)S(1)} %fusion.20), kind=kOutput, calls=%fused_computation.7 | convolution fusion | flops 1478819840 | bytes 8257536 | tf_op jit(solution)/shard_map/dot_general | solution.py:68
  193.0 0.0 all-gather.13.cloned.1.call-start
  193.0 0.5 all-gather.13.cloned.1.call-update
  193.5 0.0 all-gather.15.cloned.1.call-start
  193.6 0.5 all-gather.15.cloned.1.call-update
  194.2 0.7 all-gather.17.cloned.1.call-update
  194.9 0.0 reduce-scatter.5.cloned.1.call-start
  194.9 4.7 %reduce-scatter.3.cloned.1.call-done = bf16[128,1024]{1,0:T(8,128)(2,1)} async-done(((bf16[256,1024]{1,0:T(8,128)(2,1)}), bf16[128,1024]{1,0:T(8,128)(2,1)}) %reduce-scatter.3.cloned.1.call-update) | async-done | bytes 262160 | tf_op jit(solution)/shard_map/reduce_scatter | solution.py:70
  199.7 1.1 add_convert_fusion.1
  200.7 2.2 all_gather.28
  202.9 0.2 fusion.2
  203.1 57.0 %all-gather.13.cloned.1.call-done = bf16[1024,1408]{1,0:T(8,128)(2,1)} async-done(((bf16[128,1408]{1,0:T(8,128)(2,1)}), bf16[1024,1408]{1,0:T(8,128)(2,1)}) %all-gather.13.cloned.1.call-update) | async-done | bytes 2883600 | tf_op jit(solution)/shard_map/all_gather | solution.py:12
  260.2 2.9 fusion.16
  263.0 55.1 %all-gather.15.cloned.1.call-done = bf16[1024,1408]{1,0:T(8,128)(2,1)} async-done(((bf16[128,1408]{1,0:T(8,128)(2,1)}), bf16[1024,1408]{1,0:T(8,128)(2,1)}) %all-gather.15.cloned.1.call-update) | async-done | bytes 2883600 | tf_op jit(solution)/shard_map/all_gather | solution.py:12
  318.1 60.3 %all-gather.17.cloned.1.call-done = bf16[1408,1024]{1,0:T(8,128)(2,1)} async-done(((bf16[1408,128]{1,0:T(8,128)(2,1)}), bf16[1408,1024]{1,0:T(8,128)(2,1)}) %all-gather.17.cloned.1.call-update) | async-done | bytes 2883600 | tf_op jit(solution)/shard_map/all_gather | solution.py:42
  378.4 5.4 %convolution_convert_fusion = bf16[256,1024]{1,0:T(8,128)(2,1)} fusion(bf16[1408,1024]{1,0:T(8,128)(2,1)} %all-gather.17.cloned.1.call-done, bf16[1024,1408]{1,0:T(8,128)(2,1)} %all-gather.15.cloned.1.call-done, f32[256,1408]{1,0:T(8,128)S(1)} %fusion.16, bf16[256,1024]{1,0:T(8,128)(2,1)S(1)} %all_gather.28, f32[1024]{0:T(1024)S(1)} %copy-done.2, ...), kind=kOutput, calls=%fused_computation.6 | convolution fusion | flops 1479868416 | bytes 8262656 | tf_op jit(solution)/shard_map/dot_general | solution.py:80
  383.8 6.3 %reduce-scatter.5.cloned.1.call-done = bf16[256,512]{1,0:T(8,128)(2,1)} async-done(((bf16[256,1024]{1,0:T(8,128)(2,1)}), bf16[256,512]{1,0:T(8,128)(2,1)}) %reduce-scatter.5.cloned.1.call-update) | async-done | bytes 262160 | tf_op jit(solution)/shard_map/reduce_scatter | solution.py:81
  390.1 1.1 fusion.7
  391.2 2.5 psum.7
  393.7 1.8 fusion.9
  (16 shorter events, 0.2 us)
Async XLA Ops:
  6.5 63.0 %all-gather.7.cloned.1.call-start = ((), (), s32[]{:S(2)}) async-start(), calls=%async_computation.2 | async-start | bytes 3244032 | tf_op jit(solution)/shard_map/all_gather | solution.py:12
  7.3 122.6 %all-gather.11.cloned.1.call-start = ((), (), s32[]{:S(2)}) async-start(), calls=%async_computation.4 | async-start | bytes 3244032 | tf_op jit(solution)/shard_map/all_gather | solution.py:42
  8.0 179.5 %all-gather.9.cloned.1.call-start = ((), (), s32[]{:S(2)}) async-start(), calls=%async_computation.3 | async-start | bytes 3244032 | tf_op jit(solution)/shard_map/all_gather | solution.py:12
  8.7 190.9 %reduce-scatter.3.cloned.1.call-start = ((), (), s32[]{:S(2)}) async-start(), calls=%async_computation.5 | async-start | bytes 786432 | tf_op jit(solution)/shard_map/reduce_scatter | solution.py:70
  72.4 127.3 %copy-start = (bf16[128,1024]{1,0:T(8,128)(2,1)S(1)}, bf16[128,1024]{1,0:T(8,128)(2,1)}, u32[]{:S(2)}) copy-start(bf16[128,1024]{1,0:T(8,128)(2,1)} %param.11) | copy-start | bytes 786436
  72.4 127.3 %copy-start.1 = (bf16[256,1024]{1,0:T(8,128)(2,1)S(1)}, bf16[256,1024]{1,0:T(8,128)(2,1)}, u32[]{:S(2)}) copy-start(bf16[256,1024]{1,0:T(8,128)(2,1)} %param.12) | copy-start | bytes 1572868
  192.9 67.2 %copy-start.2 = (f32[1024]{0:T(1024)S(1)}, f32[1024]{0:T(1024)}, u32[]{:S(2)}) copy-start(f32[1024]{0:T(1024)} %param.17) | copy-start | bytes 12292
  193.0 67.2 %all-gather.13.cloned.1.call-start = ((), (), s32[]{:S(2)}) async-start(), calls=%async_computation.6 | async-start | bytes 3244032 | tf_op jit(solution)/shard_map/all_gather | solution.py:12
  193.5 124.6 %all-gather.15.cloned.1.call-start = ((), (), s32[]{:S(2)}) async-start(), calls=%async_computation.7 | async-start | bytes 3244032 | tf_op jit(solution)/shard_map/all_gather | solution.py:12
  194.1 184.3 %all-gather.17.cloned.1.call-start = ((), (), s32[]{:S(2)}) async-start(), calls=%async_computation.8 | async-start | bytes 3244032 | tf_op jit(solution)/shard_map/all_gather | solution.py:42
  194.9 195.2 %reduce-scatter.5.cloned.1.call-start = ((), (), s32[]{:S(2)}) async-start(), calls=%async_computation.9 | async-start | bytes 786432 | tf_op jit(solution)/shard_map/reduce_scatter | solution.py:81
  263.0 130.7 %copy-start.3 = (f32[512]{0:T(512)S(1)}, f32[512]{0:T(512)}, u32[]{:S(2)}) copy-start(f32[512]{0:T(512)} %param.21) | copy-start | bytes 6148
Sparse Core Ops, SparseCore 0:
  9.5 60.0 all-gather.6
  71.6 58.1 all-gather.10
  132.0 55.4 all-gather.8
  193.1 6.5 reduce-scatter.2
  201.7 58.4 all-gather.12
  262.2 55.9 all-gather.14
  320.2 58.1 all-gather.16
  384.0 6.0 reduce-scatter.4
where the time goes:
time: 403 us; the launch traced here: 402 us
  waiting for transfers between devices  359 us (89%)
  matrix products  16.5 us (4%)
  between operations  13.6 us (3%)
  blocking collectives  6.95 us (2%)
  other arithmetic  6.36 us (2%)
    all_gather x4, waiting for transfers between devices, gathered(): return lax.all_gather(part, axis, axis=dim, tiled=True)  226 us
    all_gather x2, waiting for transfers between devices, outer_weight(): return lax.all_gather(w_down, 'fs', axis=1, tiled=True)  118 us
  transfers between devices with their start and end apart: 8, of which 8 were waited for; matrix products, arithmetic and copies ran while one was open for 2% of the time, Pallas kernels for 0%

commit v1 on v0

--- a/solution.py
+++ b/solution.py
@@ -39,7 +39,7 @@
 
 
 def outer_weight(w_down):
-    return lax.all_gather(w_down, "fs", axis=1, tiled=True)
+    return jnp.concatenate(lax.all_gather(w_down, "fs"), axis=1)
 
 
 def local(

time: 403 us -> 396 us (0.983)
  waiting for transfers between devices: 359 us -> 343 us
  local copies, waits for them, and re-layouts: 0.02 us -> 6.67 us
    all_gather x2, waiting for transfers between devices: 118 us -> 107 us  [outer_weight(): return jnp.concatenate(lax.all_gather(w_down, 'fs'), axis=1)]
    reshape x0 -> x2, local copies, waits for them, and re-layouts: none -> 6.66 us  [outer_weight(): return jnp.concatenate(lax.all_gather(w_down, 'fs'), axis=1)]
    all_gather x4, waiting for transfers between devices: 226 us -> 220 us  [gathered(): return lax.all_gather(part, axis, axis=dim, tiled=True)]
  transfers between devices with their start and end apart: 8 -> 8, of which waited for: 8 -> 8; matrix products, arithmetic and copies ran while one was open for 2% -> 6% of each run, Pallas kernels for 0% -> 0%
where the time goes in v1:
time: 396 us; the launch traced here: 395 us
  waiting for transfers between devices  343 us (87%)
  matrix products  17.8 us (4%)
  between operations  13.5 us (3%)
  blocking collectives  6.95 us (2%)
  local copies, waits for them, and re-layouts  6.67 us (2%)
  other arithmetic  6.44 us (2%)
    all_gather x4, waiting for transfers between devices, gathered(): return lax.all_gather(part, axis, axis=dim, tiled=True)  220 us
    all_gather x2, waiting for transfers between devices, outer_weight(): return jnp.concatenate(lax.all_gather(w_down, 'fs'), axis=1)  107 us
    dot_general x2, matrix products, add_both(): jnp.dot(columns, pieces[0], preferred_element_type=jnp.float32)  7.96 us
  transfers between devices with their start and end apart: 8, of which 8 were waited for; matrix products, arithmetic and copies ran while one was open for 6% of the time, Pallas kernels for 0%

profile of v1, /device:TPU:0, one launch (start us, length us, event | category | flops | bytes accessed | tf_op | source)
XLA Modules:
  0.0 395.1 jit_solution(15235929821668697075)
XLA Ops:
  6.5 0.7 all-gather.17.cloned.1.call-update
  7.3 0.7 all-gather.9.cloned.1.call-update
  8.1 0.7 all-gather.11.cloned.1.call-update
  8.8 0.5 all-gather.19.cloned.1.call-update
  9.3 0.0 reduce-scatter.3.cloned.1.call-start
  9.4 1.1 fusion.10
  10.5 1.1 fusion.12
  11.6 2.3 all_gather.30
  13.9 55.7 %all-gather.17.cloned.1.call-done = bf16[11264,128]{1,0:T(8,128)(2,1)} async-done(((bf16[1408,128]{1,0:T(8,128)(2,1)}), bf16[11264,128]{1,0:T(8,128)(2,1)}) %all-gather.17.cloned.1.call-update) | async-done | bytes 2883600 | tf_op jit(solution)/shard_map/all_gather | solution.py:42
  69.6 3.3 copy.12
  72.9 54.8 %all-gather.9.cloned.1.call-done = bf16[1024,1408]{1,0:T(8,128)(2,1)} async-done(((bf16[128,1408]{1,0:T(8,128)(2,1)}), bf16[1024,1408]{1,0:T(8,128)(2,1)}) %all-gather.9.cloned.1.call-update) | async-done | bytes 2883600 | tf_op jit(solution)/shard_map/all_gather | solution.py:12
  127.7 4.0 %fusion.20 = f32[256,1408]{1,0:T(8,128)} fusion(bf16[256,1024]{1,0:T(8,128)(2,1)S(1)} %all_gather.30, bf16[1024,1408]{1,0:T(8,128)(2,1)} %all-gather.9.cloned.1.call-done), kind=kOutput, calls=%fused_computation.33 | convolution fusion | flops 738197504 | bytes 4849664 | tf_op jit(solution)/shard_map/dot_general | solution.py:32
  131.7 54.2 %all-gather.11.cloned.1.call-done = bf16[1024,1408]{1,0:T(8,128)(2,1)} async-done(((bf16[128,1408]{1,0:T(8,128)(2,1)}), bf16[1024,1408]{1,0:T(8,128)(2,1)}) %all-gather.11.cloned.1.call-update) | async-done | bytes 2883600 | tf_op jit(solution)/shard_map/all_gather | solution.py:12
  185.9 4.9 %convolution_convert_fusion.1 = bf16[256,1024]{1,0:T(8,128)(2,1)} fusion(bf16[1408,1024]{0,1:T(8,128)(2,1)S(1)} %bitcast.19, bf16[256,1024]{1,0:T(8,128)(2,1)S(1)} %all_gather.30, bf16[1024,1408]{1,0:T(8,128)(2,1)} %all-gather.11.cloned.1.call-done, f32[256,1408]{1,0:T(8,128)} %fusion.20), kind=kOutput, calls=%fused_computation.7 | convolution fusion | flops 1478819840 | bytes 8257536 | tf_op jit(solution)/shard_map/dot_general | solution.py:68
  190.7 0.0 all-gather.13.cloned.1.call-start
  190.8 0.5 all-gather.13.cloned.1.call-update
  191.4 0.7 all-gather.15.cloned.1.call-update
  192.1 0.0 reduce-scatter.5.cloned.1.call-start
  192.1 51.7 %all-gather.19.cloned.1.call-done = bf16[11264,128]{1,0:T(8,128)(2,1)} async-done(((bf16[1408,128]{1,0:T(8,128)(2,1)}), bf16[11264,128]{1,0:T(8,128)(2,1)}) %all-gather.19.cloned.1.call-update) | async-done | bytes 2883600 | tf_op jit(solution)/shard_map/all_gather | solution.py:42
  243.9 3.3 copy.13
  247.2 5.3 %reduce-scatter.3.cloned.1.call-done = bf16[128,1024]{1,0:T(8,128)(2,1)} async-done(((bf16[256,1024]{1,0:T(8,128)(2,1)}), bf16[128,1024]{1,0:T(8,128)(2,1)}) %reduce-scatter.3.cloned.1.call-update) | async-done | bytes 262160 | tf_op jit(solution)/shard_map/reduce_scatter | solution.py:70
  252.5 1.2 add_convert_fusion.1
  253.7 2.2 all_gather.35
  255.9 0.2 fusion.2
  256.1 57.0 %all-gather.13.cloned.1.call-done = bf16[1024,1408]{1,0:T(8,128)(2,1)} async-done(((bf16[128,1408]{1,0:T(8,128)(2,1)}), bf16[1024,1408]{1,0:T(8,128)(2,1)}) %all-gather.13.cloned.1.call-update) | async-done | bytes 2883600 | tf_op jit(solution)/shard_map/all_gather | solution.py:12
  313.0 4.0 %fusion.16 = f32[256,1408]{1,0:T(8,128)} fusion(bf16[1024,1408]{1,0:T(8,128)(2,1)} %all-gather.13.cloned.1.call-done, bf16[256,1024]{1,0:T(8,128)(2,1)S(1)} %all_gather.35, f32[1024]{0:T(1024)S(1)} %copy-done.1, f32[256]{0:T(256)S(1)} %add_rsqrt_fusion.1), kind=kOutput, calls=%fused_computation.27 | convolution fusion | flops 739246080 | bytes 4854784 | tf_op jit(solution)/shard_map/dot_general | solution.py:32
  317.0 54.1 %all-gather.15.cloned.1.call-done = bf16[1024,1408]{1,0:T(8,128)(2,1)} async-done(((bf16[128,1408]{1,0:T(8,128)(2,1)}), bf16[1024,1408]{1,0:T(8,128)(2,1)}) %all-gather.15.cloned.1.call-update) | async-done | bytes 2883600 | tf_op jit(solution)/shard_map/all_gather | solution.py:12
  371.2 4.9 %convolution_convert_fusion = bf16[256,1024]{1,0:T(8,128)(2,1)} fusion(bf16[1408,1024]{0,1:T(8,128)(2,1)S(1)} %bitcast.18, bf16[1024,1408]{1,0:T(8,128)(2,1)} %all-gather.15.cloned.1.call-done, f32[256,1408]{1,0:T(8,128)} %fusion.16, bf16[256,1024]{1,0:T(8,128)(2,1)S(1)} %all_gather.35, f32[1024]{0:T(1024)S(1)} %copy-done.1, f32[256]{0:T(256)S(1)} %add_rsqrt_fusion.1), kind=kOutput, calls=%fused_computation.6 | convolution fusion | flops 1479868416 | bytes 8262656 | tf_op jit(solution)/shard_map/dot_general | solution.py:80
  376.1 6.7 %reduce-scatter.5.cloned.1.call-done = bf16[256,512]{1,0:T(8,128)(2,1)} async-done(((bf16[256,1024]{1,0:T(8,128)(2,1)}), bf16[256,512]{1,0:T(8,128)(2,1)}) %reduce-scatter.5.cloned.1.call-update) | async-done | bytes 262160 | tf_op jit(solution)/shard_map/reduce_scatter | solution.py:81
  382.8 1.1 fusion.7
  384.0 2.5 psum.7
  386.4 1.8 fusion.9
  (16 shorter events, 0.2 us)
Async XLA Ops:
  6.5 63.0 %all-gather.17.cloned.1.call-start = ((), (), s32[]{:S(2)}) async-start(), calls=%async_computation.8 | async-start | bytes 3244032 | tf_op jit(solution)/shard_map/all_gather | solution.py:42
  7.3 120.5 %all-gather.9.cloned.1.call-start = ((), (), s32[]{:S(2)}) async-start(), calls=%async_computation.2 | async-start | bytes 3244032 | tf_op jit(solution)/shard_map/all_gather | solution.py:12
  8.0 177.9 %all-gather.11.cloned.1.call-start = ((), (), s32[]{:S(2)}) async-start(), calls=%async_computation.3 | async-start | bytes 3244032 | tf_op jit(solution)/shard_map/all_gather | solution.py:12
  8.7 235.1 %all-gather.19.cloned.1.call-start = ((), (), s32[]{:S(2)}) async-start(), calls=%async_computation.9 | async-start | bytes 3244032 | tf_op jit(solution)/shard_map/all_gather | solution.py:42
  9.3 243.2 %reduce-scatter.3.cloned.1.call-start = ((), (), s32[]{:S(2)}) async-start(), calls=%async_computation.4 | async-start | bytes 786432 | tf_op jit(solution)/shard_map/reduce_scatter | solution.py:70
  190.7 122.3 %all-gather.13.cloned.1.call-start = ((), (), s32[]{:S(2)}) async-start(), calls=%async_computation.5 | async-start | bytes 3244032 | tf_op jit(solution)/shard_map/all_gather | solution.py:12
  191.3 179.8 %all-gather.15.cloned.1.call-start = ((), (), s32[]{:S(2)}) async-start(), calls=%async_computation.6 | async-start | bytes 3244032 | tf_op jit(solution)/shard_map/all_gather | solution.py:12
  192.1 190.8 %reduce-scatter.5.cloned.1.call-start = ((), (), s32[]{:S(2)}) async-start(), calls=%async_computation.7 | async-start | bytes 786432 | tf_op jit(solution)/shard_map/reduce_scatter | solution.py:81
  243.8 8.7 %copy-start = (bf16[128,1024]{1,0:T(8,128)(2,1)S(1)}, bf16[128,1024]{1,0:T(8,128)(2,1)}, u32[]{:S(2)}) copy-start(bf16[128,1024]{1,0:T(8,128)(2,1)} %param.11) | copy-start | bytes 786436
  243.9 69.2 %copy-start.1 = (f32[1024]{0:T(1024)S(1)}, f32[1024]{0:T(1024)}, u32[]{:S(2)}) copy-start(f32[1024]{0:T(1024)} %param.17) | copy-start | bytes 12292
  371.2 15.3 %copy-start.2 = (f32[512]{0:T(512)S(1)}, f32[512]{0:T(512)}, u32[]{:S(2)}) copy-start(f32[512]{0:T(512)} %param.21) | copy-start | bytes 6148
Sparse Core Ops, SparseCore 0:
  9.5 60.0 all-gather.16
  71.8 55.9 all-gather.8
  129.9 55.9 all-gather.10
  187.9 55.9 all-gather.18
  245.9 6.5 reduce-scatter.2
  254.6 58.4 all-gather.12
  315.2 55.9 all-gather.14
  376.2 6.5 reduce-scatter.4
